TPU v7x, 256 devices: a whole 4x4x8 slice. The times are simulated.
256 devices in a mesh: rep: 2 (over z_hi), fs: 16 (over z_lo, x), tp: 8 (over y, core).
Axes of the slice: x: 4, y: 4, z: 8 (z_hi: 2, z_lo: 4; z = z_hi * 4 + z_lo), core: 2. Of those that a mesh axis runs over, the one named last changes fastest.
Arguments:
- tokens: bfloat16 [32768, 2048], P(('rep', 'fs'), 'tp'), may hold values from -6 to 6
- mix_in_gain: bfloat16 [2048], replicated, may hold values from 0.099609375 to 1.8984375
- bgate_weight: bfloat16 [2048, 2048], P('fs', 'tp'), may hold values from -0.125 to 0.125
- cgate_weight: bfloat16 [2048, 2048], P('fs', 'tp'), may hold values from -0.125 to 0.125
- value_weight: bfloat16 [2048, 2048], P('fs', 'tp'), may hold values from -0.125 to 0.125
- conv_taps: bfloat16 [3, 2048], replicated, may hold values from -3 to 3
- out_weight: bfloat16 [2048, 2048], P('tp', 'fs'), may hold values from -0.41984465 to 0.41984465
- mix_out_gain: bfloat16 [2048], replicated, may hold values from 0.099609375 to 1.8984375
- ffn_in_gain: bfloat16 [2048], replicated, may hold values from 0.099609375 to 1.8984375
- up_weight: bfloat16 [2048, 8192], P('fs', 'tp'), may hold values from -0.125 to 0.125
- down_weight: bfloat16 [8192, 2048], P('tp', 'fs'), may hold values from -0.20992233 to 0.20992233
- ffn_out_gain: bfloat16 [2048], replicated, may hold values from 0.099609375 to 1.8984375
Outputs:
- result: bfloat16 [32768, 2048], P(('rep', 'fs'), 'tp')
All inputs are finite; a program needn't handle non-finite values.
Results may differ from a plain program's by a relative error of at most 0.02.
Values may be sent and summed in bfloat16 or wider, within the bound.
A program may use at most 128 MiB of HBM per device.

v0:
```python
import jax
import jax.numpy as jnp
from jax import lax
from jax.sharding import Mesh
from jax.sharding import PartitionSpec as P

LEN = 256
FS = ("fs_0", "fs_1")
REP_FS = ("rep", "fs_0", "fs_1")
epsilon = 1e-06


def in_order(pieces, dim):
    pieces = jnp.moveaxis(pieces, 0, dim)
    shape = pieces.shape
    return pieces.reshape(*shape[:dim], shape[dim] * shape[dim + 1], *shape[dim + 2 :])


def from_everyone(x, axis):
    length = lax.axis_size(axis)
    return lax.all_to_all(jnp.broadcast_to(x[None], (length, *x.shape)), axis, 0, 0, tiled=True)


def gathered_copies(x, axis, dim):
    return in_order(from_everyone(x, axis), dim)


def in_blocks(x, dim, length):
    before, after = (x.shape[:dim], x.shape[dim + 1 :])
    return jnp.moveaxis(x.reshape(*before, length, -1, *after), dim, 0)


def sent_and_summed(x, axis, dim):
    pieces = in_blocks(x, dim, lax.axis_size(axis))
    arrived = lax.all_to_all(pieces, axis, split_axis=0, concat_axis=0, tiled=True)
    return arrived.astype(jnp.float32).sum(axis=0)


def of_everyone(x, axis):
    everything = from_everyone(x, axis)
    return jnp.sum(everything, axis=0)


def all_blocks(x, axes, order):
    pieces = x
    for k in order:
        pieces = lax.all_gather(pieces, axes[k])
    done = order[::-1]
    back = [done.index(k) for k in range(len(axes))]
    pieces = pieces.transpose(*back, *range(len(axes), pieces.ndim))
    return pieces.reshape(-1, *x.shape)


def whole_of(x, axes, order, dim):
    return in_order(all_blocks(x, axes, order), dim)


def normalize(rows, gain):
    rows = rows.astype(jnp.float32)
    factor = lax.rsqrt(jnp.mean(rows * rows, axis=-1, keepdims=True) + epsilon)
    return rows * factor * gain.astype(jnp.float32)


def convolve(inner, taps):
    seqs = inner.reshape(-1, LEN, inner.shape[1])
    padded = jnp.pad(seqs, ((0, 0), (1, 1), (0, 0)))
    weights = taps.astype(jnp.float32)
    out = weights[0] * padded[:, :-2] + weights[1] * padded[:, 1:-1] + weights[2] * padded[:, 2:]
    return out.reshape(inner.shape)


def body(
    tokens,
    mix_in_gain,
    bgate_weight,
    cgate_weight,
    value_weight,
    conv_taps,
    out_weight,
    mix_out_gain,
    ffn_in_gain,
    up_weight,
    down_weight,
    ffn_out_gain,
):
    column = lax.axis_index("tp")
    own_width = tokens.shape[1]
    first = column * own_width
    full_width = mix_in_gain.shape[0]
    whole = lax.all_gather(tokens, "tp", axis=1, tiled=True)
    normed = normalize(whole, mix_in_gain).astype(jnp.bfloat16)

    def add_rows(piece):
        return jnp.dot(normed, piece, preferred_element_type=jnp.float32)

    bgate = add_rows(gathered_copies(bgate_weight, FS, 0))
    cgate = add_rows(gathered_copies(cgate_weight, FS, 0))
    value = add_rows(gathered_copies(value_weight, FS, 0))
    bgate = bgate.astype(jnp.bfloat16)
    cgate = cgate.astype(jnp.bfloat16)
    value = value.astype(jnp.bfloat16)
    channels = bgate.shape[1]
    own_taps = lax.dynamic_slice_in_dim(conv_taps, column * channels, channels, 1)
    inner = cgate.astype(jnp.float32) * value.astype(jnp.float32)
    gated = (bgate.astype(jnp.float32) * convolve(inner, own_taps)).astype(jnp.bfloat16)
    partial_mix = jnp.dot(
        gated, gathered_copies(out_weight, FS, 1), preferred_element_type=jnp.float32
    )
    mixed = sent_and_summed(partial_mix.astype(jnp.bfloat16), "tp", 1)
    power = of_everyone(jnp.sum(mixed * mixed, axis=1), "tp")
    gain_own = lax.dynamic_slice_in_dim(mix_out_gain, first, own_width, 0).astype(jnp.float32)
    scaled = mixed * lax.rsqrt(power[:, None] / full_width + epsilon) * gain_own
    resid_own = (tokens.astype(jnp.float32) + scaled).astype(jnp.bfloat16)
    resid = lax.all_gather(resid_own, "tp", axis=1, tiled=True)
    second = normalize(resid, ffn_in_gain).astype(jnp.bfloat16)
    lifted = jnp.dot(second, whole_of(up_weight, FS, (0, 1), 0), preferred_element_type=jnp.float32)
    active = jnp.square(jnp.maximum(lifted, 0.0)).astype(jnp.bfloat16)
    partial_ffn = jnp.dot(
        active, whole_of(down_weight, FS, (0, 1), 1), preferred_element_type=jnp.float32
    )
    ffn = sent_and_summed(partial_ffn.astype(jnp.bfloat16), "tp", 1)
    ffn_energy = of_everyone(jnp.sum(ffn * ffn, axis=1), "tp")
    out_gain = lax.dynamic_slice_in_dim(ffn_out_gain, first, own_width, 0).astype(jnp.float32)
    closing = ffn * lax.rsqrt(ffn_energy[:, None] / full_width + epsilon) * out_gain
    return (resid_own.astype(jnp.float32) + closing).astype(jnp.bfloat16)


def solution(mesh):
    torus = Mesh(
        mesh.devices.reshape(mesh.shape["rep"], 4, 4, mesh.shape["tp"]),
        ("rep", "fs_0", "fs_1", "tp"),
    )
    return jax.shard_map(
        body,
        mesh=torus,
        in_specs=(
            P(REP_FS, "tp"),
            P(),
            P(FS, "tp"),
            P(FS, "tp"),
            P(FS, "tp"),
            P(),
            P("tp", FS),
            P(),
            P(),
            P(FS, "tp"),
            P("tp", FS),
            P(),
        ),
        out_specs=P(REP_FS, "tp"),
        check_vma=False,
    )
```

profile of v0, /device:TPU:1, one launch (start us, length us, event | category | flops | bytes accessed | tf_op | source)
XLA Modules:
  0.0 391.8 jit_solution(6726258593251835402)
XLA Ops:
  6.5 0.0 all-gather.19.cloned.1.call-start
  6.5 0.7 all-gather.19.cloned.1.call-update
  7.3 0.0 copy-start.5
  7.3 0.0 all-gather.15.cloned.1.call-start
  7.3 0.7 all-gather.15.cloned.1.call-update
  8.0 0.0 all-gather.11.cloned.1.call-start
  8.1 0.7 all-gather.11.cloned.1.call-update
  8.8 0.0 all-gather.21.cloned.1.call-start
  8.8 36.9 %all-gather.19.cloned.1.call-done = bf16[4096,128]{1,0:T(8,128)(2,1)} async-done(((bf16[1024,128]{1,0:T(8,128)(2,1)}), bf16[4096,128]{1,0:T(8,128)(2,1)}) %all-gather.19.cloned.1.call-update) | async-done | bytes 1048592 | tf_op jit(solution)/shard_map/all_gather | solution.py:47
  45.7 0.0 all-gather.21.cloned.1.call-update
  45.8 0.9 broadcast_in_dim.13
  46.7 0.0 copy-start.4
  46.7 40.9 %all_to_all.42 = bf16[16,128,256]{2,1,0:T(8,128)(2,1)S(1)} all-to-all(bf16[16,128,256]{2,1,0:T(8,128)(2,1)S(1)} %broadcast_in_dim.13), channel_id=1, replica_groups=mesh['rep'=2,'fs_0'=4,'fs_1'=4,'tp'=8] {'fs_0','fs_1'}, dimensions={0} | all-to-all | bytes 2097152 | tf_op jit(solution)/shard_map/all_to_all | solution.py:21
  87.6 0.0 copy-done.3
  87.6 1.1 broadcast_in_dim.14
  88.7 9.8 %all-to-all-start.2 = ((bf16[16,128,256]{2,1,0:T(8,128)(2,1)}), bf16[16,128,256]{2,1,0:T(8,128)(2,1)S(1)}, u32[]{:S(2)}, u32[]{:S(2)}) async-start(bf16[16,128,256]{2,1,0:T(8,128)(2,1)} %broadcast_in_dim.14), calls=%async_computation.2 | async-start | bytes 2097152 | tf_op jit(solution)/shard_map/all_to_all | solution.py:21
  98.5 0.1 copy.31
  98.6 21.9 %all-to-all-done.2 = bf16[16,128,256]{2,1,0:T(8,128)(2,1)S(1)} async-done(((bf16[16,128,256]{2,1,0:T(8,128)(2,1)}), bf16[16,128,256]{2,1,0:T(8,128)(2,1)S(1)}, u32[]{:S(2)}, u32[]{:S(2)}) %all-to-all-start.2) | async-done | bytes 1048608 | tf_op jit(solution)/shard_map/all_to_all | solution.py:21
  120.5 1.1 broadcast_in_dim.15
  121.5 7.9 %all-to-all-start.3 = ((bf16[16,256,128]{1,2,0:T(8,128)(2,1)}), bf16[16,256,128]{1,2,0:T(8,128)(2,1)S(1)}, u32[]{:S(2)}, u32[]{:S(2)}) async-start(bf16[16,256,128]{1,2,0:T(8,128)(2,1)} %broadcast_in_dim.15), calls=%async_computation.3 | async-start | bytes 2097152 | tf_op jit(solution)/shard_map/all_to_all | solution.py:21
  129.4 0.7 dynamic-slice_convert_fusion
  130.1 21.5 %all-to-all-done.3 = bf16[16,256,128]{1,2,0:T(8,128)(2,1)S(1)} async-done(((bf16[16,256,128]{1,2,0:T(8,128)(2,1)}), bf16[16,256,128]{1,2,0:T(8,128)(2,1)S(1)}, u32[]{:S(2)}, u32[]{:S(2)}) %all-to-all-start.3) | async-done | bytes 1048608 | tf_op jit(solution)/shard_map/all_to_all | solution.py:21
  151.6 0.0 copy-done.4
  151.6 1.2 broadcast_in_dim.12
  152.8 7.8 %all-to-all-start = ((bf16[16,128,256]{2,1,0:T(8,128)(2,1)}), bf16[16,128,256]{2,1,0:T(8,128)(2,1)}, u32[]{:S(2)}, u32[]{:S(2)}) async-start(bf16[16,128,256]{2,1,0:T(8,128)(2,1)} %broadcast_in_dim.12), calls=%async_computation | async-start | bytes 2097152 | tf_op jit(solution)/shard_map/all_to_all | solution.py:21
  160.6 0.0 all-gather.17.cloned.1.call-start
  160.7 0.0 copy-done.6
  160.7 0.0 all-gather.15.cloned.1.call-done
  160.7 0.5 all-gather.17.cloned.1.call-update
  161.2 0.0 all-gather.11.cloned.1.call-done
  161.2 3.2 fusion
  164.5 0.3 copy-done.1
  164.7 1.3 fusion.13
  166.0 1.3 fusion.12
  167.4 0.3 multiply_add_fusion
  167.7 15.1 %all-to-all-done = bf16[16,128,256]{2,1,0:T(8,128)(2,1)} async-done(((bf16[16,128,256]{2,1,0:T(8,128)(2,1)}), bf16[16,128,256]{2,1,0:T(8,128)(2,1)}, u32[]{:S(2)}, u32[]{:S(2)}) %all-to-all-start) | async-done | bytes 1048608 | tf_op jit(solution)/shard_map/all_to_all | solution.py:21
  182.8 8.8 %convolution_convert_fusion = bf16[1024,2048]{1,0:T(8,128)(2,1)} fusion(bf16[256,2048]{0,1:T(8,128)(2,1)S(1)} %bitcast.55, f32[1024,256]{1,0:T(8,128)S(1)} %bitcast.58, bf16[2048,256]{1,0:T(8,128)(2,1)} %bitcast, bf16[1024,2048]{1,0:T(8,128)(2,1)} %all-gather.11.cloned.1.call-done, f32[2048]{0:T(1024)S(1)} %convert_element_type.79, ...), kind=kOutput, calls=%fused_computation.18 | convolution fusion | flops 2159017984 | bytes 11546624 | tf_op jit(solution)/shard_map/dot_general | solution.py:106
  191.7 2.5 copy.46
  194.1 56.0 %all_to_all.43 = bf16[8,1024,256]{2,1,0:T(8,128)(2,1)S(1)} all-to-all(bf16[8,1024,256]{2,1,0:T(8,128)(2,1)S(1)} %bitcast.44), channel_id=1, replica_groups=mesh['rep'=2,'fs_0'=4,'fs_1'=4,'tp'=8] {'tp'}, dimensions={0} | all-to-all | bytes 8388608 | tf_op jit(solution)/shard_map/all_to_all | solution.py:35
  250.2 0.6 convert_reduce_fusion.1
  250.8 0.2 multiply_reduce_fusion.1
  251.0 0.6 broadcast_in_dim.16
  251.6 4.2 %all-to-all-start.5 = ((f32[8,1,1024]{2,1,0:T(1,128)}), f32[8,1,1024]{2,1,0:T(1,128)S(1)}, u32[]{:S(2)}, u32[]{:S(2)}) async-start(f32[8,1,1024]{2,1,0:T(1,128)} %broadcast_in_dim.16), calls=%async_computation.5 | async-start | bytes 65536 | tf_op jit(solution)/shard_map/all_to_all | solution.py:21
  255.8 0.0 all-gather.13.cloned.1.call-start
  255.8 0.8 dynamic-slice_convert_fusion.2
  256.6 4.0 %all-to-all-done.5 = f32[8,1,1024]{2,1,0:T(1,128)S(1)} async-done(((f32[8,1,1024]{2,1,0:T(1,128)}), f32[8,1,1024]{2,1,0:T(1,128)S(1)}, u32[]{:S(2)}, u32[]{:S(2)}) %all-to-all-start.5) | async-done | bytes 32800 | tf_op jit(solution)/shard_map/all_to_all | solution.py:21
  260.6 1.1 add_convert_fusion.1
  261.7 0.0 all-gather.13.cloned.1.call-update
  261.7 0.0 all-gather.21.cloned.1.call-done
  261.8 4.5 %copy.35 = bf16[4,4,1024,128]{3,2,1,0:T(8,128)(2,1)} copy(bf16[4,4,1024,128]{3,2,0,1:T(8,128)(2,1)} %bitcast.47) | data formatting | bytes 8388608 | tf_op jit(solution)/shard_map/transpose | solution.py:50
  266.3 6.4 %copy.36 = bf16[1024,16,128]{0,2,1:T(8,128)(2,1)} copy(bf16[1024,16,128]{2,0,1:T(8,128)(2,1)} %bitcast.45) | data formatting | bytes 8388608 | tf_op jit(solution)/shard_map/transpose | solution.py:14
  272.7 5.0 %copy.34 = bf16[4,4,128,1024]{3,2,1,0:T(8,128)(2,1)} copy(bf16[4,4,128,1024]{3,2,0,1:T(8,128)(2,1)} %bitcast.48) | data formatting | bytes 8388608 | tf_op jit(solution)/shard_map/transpose | solution.py:50
  277.7 22.9 %all-gather.13.cloned.1.call-done = bf16[1024,2048]{1,0:T(8,128)(2,1)} async-done(((bf16[1024,256]{1,0:T(8,128)(2,1)}), bf16[1024,2048]{1,0:T(8,128)(2,1)}) %all-gather.13.cloned.1.call-update) | async-done | bytes 4194320 | tf_op jit(solution)/shard_map/all_gather | solution.py:114
  300.6 3.1 fusion.3
  303.7 14.6 %convolution_convert_fusion.1 = bf16[1024,2048]{1,0:T(8,128)(2,1)} fusion(bf16[1024,2048]{0,1:T(8,128)(2,1)} %bitcast.49, bf16[2048,1024]{1,0:T(8,128)(2,1)} %bitcast.50, bf16[1024,2048]{1,0:T(8,128)(2,1)} %all-gather.13.cloned.1.call-done, f32[2048]{0:T(1024)S(1)} %convert_element_type.95, f32[1024]{0:T(1024)S(1)} %add_rsqrt_fusion.1), kind=kOutput, calls=%fused_computation.19 | convolution fusion | flops 8603566080 | bytes 16789504 | tf_op jit(solution)/shard_map/dot_general | solution.py:118
  318.3 2.5 copy.45
  320.8 52.6 %all_to_all.44 = bf16[8,1024,256]{2,1,0:T(8,128)(2,1)S(1)} all-to-all(bf16[8,1024,256]{2,1,0:T(8,128)(2,1)S(1)} %bitcast.46), channel_id=1, replica_groups=mesh['rep'=2,'fs_0'=4,'fs_1'=4,'tp'=8] {'tp'}, dimensions={0} | all-to-all | bytes 8388608 | tf_op jit(solution)/shard_map/all_to_all | solution.py:35
  373.4 0.6 convert_reduce_fusion
  374.0 0.2 multiply_reduce_fusion
  374.2 0.6 broadcast_in_dim.17
  374.8 4.3 %all-to-all-start.7 = ((f32[8,1,1024]{2,1,0:T(1,128)}), f32[8,1,1024]{2,1,0:T(1,128)S(1)}, u32[]{:S(2)}, u32[]{:S(2)}) async-start(f32[8,1,1024]{2,1,0:T(1,128)} %broadcast_in_dim.17), calls=%async_computation.7 | async-start | bytes 65536 | tf_op jit(solution)/shard_map/all_to_all | solution.py:21
  379.1 0.8 dynamic-slice_convert_fusion.1
  379.9 4.0 %all-to-all-done.7 = f32[8,1,1024]{2,1,0:T(1,128)S(1)} async-done(((f32[8,1,1024]{2,1,0:T(1,128)}), f32[8,1,1024]{2,1,0:T(1,128)S(1)}, u32[]{:S(2)}, u32[]{:S(2)}) %all-to-all-start.7) | async-done | bytes 32800 | tf_op jit(solution)/shard_map/all_to_all | solution.py:21
  383.9 1.1 add_convert_fusion
  (20 shorter events, 0.1 us)
Async XLA Ops:
  6.5 81.1 %copy-start.3 = (bf16[128,256]{1,0:T(8,128)(2,1)S(1)}, bf16[128,256]{1,0:T(8,128)(2,1)}, u32[]{:S(2)}) copy-start(bf16[128,256]{1,0:T(8,128)(2,1)} %param.16) | copy-start | bytes 196612
  6.5 39.2 %all-gather.19.cloned.1.call-start = ((), (), s32[]{:S(2)}) async-start(), calls=%async_computation.12 | async-start | bytes 1310720 | tf_op jit(solution)/shard_map/all_gather | solution.py:47
  7.3 91.2 %copy-start.5 = (bf16[256,128]{1,0:T(8,128)(2,1)S(1)}, bf16[256,128]{1,0:T(8,128)(2,1)}, u32[]{:S(2)}) copy-start(bf16[256,128]{1,0:T(8,128)(2,1)} %param.18) | copy-start | bytes 196612
  7.3 153.4 %all-gather.15.cloned.1.call-start = ((), (), s32[]{:S(2)}) async-start(), calls=%async_computation.10 | async-start | bytes 1310720 | tf_op jit(solution)/shard_map/all_gather | solution.py:47
  8.0 153.2 %all-gather.11.cloned.1.call-start = ((), (), s32[]{:S(2)}) async-start(), calls=%async_computation.8 | async-start | bytes 4718592 | tf_op jit(solution)/shard_map/all_gather | solution.py:90
  8.8 253.0 %all-gather.21.cloned.1.call-start = ((), (), s32[]{:S(2)}) async-start(), calls=%async_computation.13 | async-start | bytes 5242880 | tf_op jit(solution)/shard_map/all_gather | solution.py:47
  46.7 104.9 %copy-start.4 = (bf16[128,256]{1,0:T(8,128)(2,1)S(1)}, bf16[128,256]{1,0:T(8,128)(2,1)}, u32[]{:S(2)}) copy-start(bf16[128,256]{1,0:T(8,128)(2,1)} %param.14) | copy-start | bytes 196612
  88.7 72.0 %copy-start.6 = (bf16[2048]{0:T(1024)(128)(2,1)S(1)}, bf16[2048]{0:T(1024)(128)(2,1)}, u32[]{:S(2)}) copy-start(bf16[2048]{0:T(1024)(128)(2,1)} %param.13) | copy-start | bytes 12292
  88.7 31.8 %all-to-all-start.2 = ((bf16[16,128,256]{2,1,0:T(8,128)(2,1)}), bf16[16,128,256]{2,1,0:T(8,128)(2,1)S(1)}, u32[]{:S(2)}, u32[]{:S(2)}) async-start(bf16[16,128,256]{2,1,0:T(8,128)(2,1)} %broadcast_in_dim.14), calls=%async_computation.2 | async-start | bytes 2097152 | tf_op jit(solution)/shard_map/all_to_all | solution.py:21
  121.5 30.1 %all-to-all-start.3 = ((bf16[16,256,128]{1,2,0:T(8,128)(2,1)}), bf16[16,256,128]{1,2,0:T(8,128)(2,1)S(1)}, u32[]{:S(2)}, u32[]{:S(2)}) async-start(bf16[16,256,128]{1,2,0:T(8,128)(2,1)} %broadcast_in_dim.15), calls=%async_computation.3 | async-start | bytes 2097152 | tf_op jit(solution)/shard_map/all_to_all | solution.py:21
  152.8 30.1 %all-to-all-start = ((bf16[16,128,256]{2,1,0:T(8,128)(2,1)}), bf16[16,128,256]{2,1,0:T(8,128)(2,1)}, u32[]{:S(2)}, u32[]{:S(2)}) async-start(bf16[16,128,256]{2,1,0:T(8,128)(2,1)} %broadcast_in_dim.12), calls=%async_computation | async-start | bytes 2097152 | tf_op jit(solution)/shard_map/all_to_all | solution.py:21
  160.6 112.1 %all-gather.17.cloned.1.call-start = ((), (), s32[]{:S(2)}) async-start(), calls=%async_computation.11 | async-start | bytes 5242880 | tf_op jit(solution)/shard_map/all_gather | solution.py:47
  161.2 3.5 copy-start.1
  250.2 10.5 %copy-start.2 = (bf16[1024,256]{1,0:T(8,128)(2,1)S(1)}, bf16[1024,256]{1,0:T(8,128)(2,1)}, u32[]{:S(2)}) copy-start(bf16[1024,256]{1,0:T(8,128)(2,1)} %param.12) | copy-start | bytes 1572868
  250.2 11.5 %copy-start.7 = (bf16[2048]{0:T(1024)(128)(2,1)S(1)}, bf16[2048]{0:T(1024)(128)(2,1)}, u32[]{:S(2)}) copy-start(bf16[2048]{0:T(1024)(128)(2,1)} %param.20) | copy-start | bytes 12292
  251.6 9.0 %all-to-all-start.5 = ((f32[8,1,1024]{2,1,0:T(1,128)}), f32[8,1,1024]{2,1,0:T(1,128)S(1)}, u32[]{:S(2)}, u32[]{:S(2)}) async-start(f32[8,1,1024]{2,1,0:T(1,128)} %broadcast_in_dim.16), calls=%async_computation.5 | async-start | bytes 65536 | tf_op jit(solution)/shard_map/all_to_all | solution.py:21
  255.8 44.7 %all-gather.13.cloned.1.call-start = ((), (), s32[]{:S(2)}) async-start(), calls=%async_computation.9 | async-start | bytes 4718592 | tf_op jit(solution)/shard_map/all_gather | solution.py:114
  373.4 10.5 %copy-start = (bf16[1024,256]{1,0:T(8,128)(2,1)S(1)}, bf16[1024,256]{1,0:T(8,128)(2,1)}, u32[]{:S(2)}) copy-start(bf16[1024,256]{1,0:T(8,128)(2,1)} %add_convert_fusion.1) | copy-start | bytes 1572868
  374.8 9.0 %all-to-all-start.7 = ((f32[8,1,1024]{2,1,0:T(1,128)}), f32[8,1,1024]{2,1,0:T(1,128)S(1)}, u32[]{:S(2)}, u32[]{:S(2)}) async-start(f32[8,1,1024]{2,1,0:T(1,128)} %broadcast_in_dim.17), calls=%async_computation.7 | async-start | bytes 65536 | tf_op jit(solution)/shard_map/all_to_all | solution.py:21
Sparse Core Ops, SparseCore 0:
  9.1 36.5 all-gather.18
  47.5 43.0 all-gather.14
  92.5 42.0 all-gather.10
  136.3 62.9 all-gather.20
  200.9 51.1 all-gather.16
  261.8 38.7 all-gather.12
where the time goes:
time: 393 us; the launch traced here: 392 us
  blocking collectives  150 us (38%)
  waiting for transfers between devices  129 us (33%)
  starting transfers between devices  34.2 us (9%)
  local copies, waits for them, and re-layouts  26.7 us (7%)
  matrix products  26.1 us (7%)
  between operations  13.7 us (3%)
  other arithmetic  12.6 us (3%)
    all_to_all x2, blocking collectives, sent_and_summed(): lax.all_to_all(pieces, axis, split_axis=0, concat_axis=0, tiled=True)  109 us
    all_to_all x5, waiting for transfers between devices, from_everyone(): lax.all_to_all(jnp.broadcast_to(x[None], (length, *x.shape)), axis, 0, 0,...  66.4 us
    all_to_all x1, blocking collectives, from_everyone(): lax.all_to_all(jnp.broadcast_to(x[None], (length, *x.shape)), axis, 0, 0,...  40.9 us
    all_gather x4, waiting for transfers between devices, all_blocks(): pieces = lax.all_gather(pieces, axes[k])  37 us
    all_to_all x5, starting transfers between devices, from_everyone(): lax.all_to_all(jnp.broadcast_to(x[None], (length, *x.shape)), axis, 0, 0,...  34 us
    all_gather x1, waiting for transfers between devices, body(): resid = lax.all_gather(resid_own, 'tp', axis=1, tiled=True)  22.9 us
    dot_general x1, matrix products, body(): jnp.dot(active, whole_of(down_weight, FS, (0, 1), 1), preferred_element_t...  14.6 us
    transpose x2, local copies, waits for them, and re-layouts, all_blocks(): pieces = pieces.transpose(*back, *range(len(axes), pieces.ndim))  9.5 us
  transfers between devices with their start and end apart: 11, of which 7 were waited for; matrix products, arithmetic and copies ran while one was open for 11% of the time, Pallas kernels for 0%

commit v1 on v0

--- a/solution.py
+++ b/solution.py
@@ -111,7 +111,37 @@
     gain_own = lax.dynamic_slice_in_dim(mix_out_gain, first, own_width, 0).astype(jnp.float32)
     scaled = mixed * lax.rsqrt(power[:, None] / full_width + epsilon) * gain_own
     resid_own = (tokens.astype(jnp.float32) + scaled).astype(jnp.bfloat16)
-    resid = lax.all_gather(resid_own, "tp", axis=1, tiled=True)
+    state_now = lax.axis_size("tp")
+    block_last = lax.axis_index("tp")
+    response, a_next, main = (state_now, block_last, resid_own.shape[1])
+    items = []
+    hop_no = 0
+    while hop_no < response:
+        items.append((hop_no, (hop_no + 1) % response))
+        hop_no = hop_no + 1
+    kept_rows = []
+    hop_no = 0
+    while hop_no < response:
+        kept_rows.append((hop_no, (hop_no - 1) % response))
+        hop_no += 1
+    resid = jnp.zeros(
+        (*resid_own.shape[:1], response * main, *resid_own.shape[1 + 1 :]), resid_own.dtype
+    )
+    resid = lax.dynamic_update_slice_in_dim(resid, resid_own, a_next * main, axis=1)
+    y1 = parts_out = resid_own
+    res = response // 2
+    src_i = 1
+    while src_i < res + 1:
+        y1 = lax.ppermute(y1, axis_name="tp", perm=items)
+        resid = lax.dynamic_update_slice_in_dim(
+            resid, y1, (a_next - src_i) % response * main, axis=1
+        )
+        if src_i < response - res:
+            parts_out = lax.ppermute(parts_out, axis_name="tp", perm=kept_rows)
+            resid = lax.dynamic_update_slice_in_dim(
+                resid, parts_out, (a_next + src_i) % response * main, axis=1
+            )
+        src_i += 1
     second = normalize(resid, ffn_in_gain).astype(jnp.bfloat16)
     lifted = jnp.dot(second, whole_of(up_weight, FS, (0, 1), 0), preferred_element_type=jnp.float32)
     active = jnp.square(jnp.maximum(lifted, 0.0)).astype(jnp.bfloat16)

time: 393 us -> 406 us (1.033)
  waiting for transfers between devices: 129 us -> 119 us
  starting transfers between devices: 34.2 us -> 43.1 us
  local copies, waits for them, and re-layouts: 26.7 us -> 35.4 us
    all_gather x1 -> x0, waiting for transfers between devices: 22.9 us -> none  [body(): resid = lax.all_gather(resid_own, 'tp', axis=1, tiled=True)]
    ppermute x0 -> x7, waiting for transfers between devices: none -> 13.4 us  [the longest x4 11.2 us: body(): y1 = lax.ppermute(y1, axis_name='tp', perm=items)]
    ppermute x0 -> x7, starting transfers between devices: none -> 8.96 us  [the longest x4 5.94 us: body(): y1 = lax.ppermute(y1, axis_name='tp', perm=items)]
    dynamic_update_slice x0 -> x7, local copies, waits for them, and re-layouts: none -> 6.2 us  [the longest x4 3.49 us: body(): lax.dynamic_update_slice_in_dim(resid, y1, (a_next - src_i) % response *...]
    all_to_all x2, blocking collectives: 109 us -> 114 us  [sent_and_summed(): lax.all_to_all(pieces, axis, split_axis=0, concat_axis=0, tiled=True)]
  transfers between devices with their start and end apart: 11 -> 17, of which waited for: 7 -> 10; matrix products, arithmetic and copies ran while one was open for 11% -> 12% of each run, Pallas kernels for 0% -> 0%
where the time goes in v1:
time: 406 us; the launch traced here: 404 us
  blocking collectives  154 us (38%)
  waiting for transfers between devices  119 us (29%)
  starting transfers between devices  43.1 us (11%)
  local copies, waits for them, and re-layouts  35.4 us (9%)
  matrix products  26.1 us (6%)
  between operations  13.4 us (3%)
  other arithmetic  12.6 us (3%)
    all_to_all x2, blocking collectives, sent_and_summed(): lax.all_to_all(pieces, axis, split_axis=0, concat_axis=0, tiled=True)  114 us
    all_to_all x5, waiting for transfers between devices, from_everyone(): lax.all_to_all(jnp.broadcast_to(x[None], (length, *x.shape)), axis, 0, 0,...  66.5 us
    all_to_all x1, blocking collectives, from_everyone(): lax.all_to_all(jnp.broadcast_to(x[None], (length, *x.shape)), axis, 0, 0,...  40.9 us
    all_gather x4, waiting for transfers between devices, all_blocks(): pieces = lax.all_gather(pieces, axes[k])  37 us
    all_to_all x5, starting transfers between devices, from_everyone(): lax.all_to_all(jnp.broadcast_to(x[None], (length, *x.shape)), axis, 0, 0,...  34 us
    dot_general x1, matrix products, body(): jnp.dot(active, whole_of(down_weight, FS, (0, 1), 1), preferred_element_t...  14.6 us
    ppermute x4, waiting for transfers between devices, body(): y1 = lax.ppermute(y1, axis_name='tp', perm=items)  11.2 us
    transpose x2, local copies, waits for them, and re-layouts, all_blocks(): pieces = pieces.transpose(*back, *range(len(axes), pieces.ndim))  9.34 us
  transfers between devices with their start and end apart: 17, of which 10 were waited for; matrix products, arithmetic and copies ran while one was open for 12% of the time, Pallas kernels for 0%

profile of v1, /device:TPU:1, one launch (start us, length us, event | category | flops | bytes accessed | tf_op | source)
XLA Modules:
  0.0 404.4 jit_solution(9851091496327775370)
XLA Ops:
  6.5 0.7 all-gather.16.cloned.1.call-update
  7.3 0.7 all-gather.12.cloned.1.call-update
  8.1 0.7 all-gather.10.cloned.1.call-update
  8.8 36.9 %all-gather.16.cloned.1.call-done = bf16[4096,128]{1,0:T(8,128)(2,1)} async-done(((bf16[1024,128]{1,0:T(8,128)(2,1)}), bf16[4096,128]{1,0:T(8,128)(2,1)}) %all-gather.16.cloned.1.call-update) | async-done | bytes 1048592 | tf_op jit(solution)/shard_map/all_gather | solution.py:47
  45.8 0.9 broadcast_in_dim.15
  46.7 40.9 %all_to_all.42 = bf16[16,128,256]{2,1,0:T(8,128)(2,1)S(1)} all-to-all(bf16[16,128,256]{2,1,0:T(8,128)(2,1)S(1)} %broadcast_in_dim.15), channel_id=1, replica_groups=mesh['rep'=2,'fs_0'=4,'fs_1'=4,'tp'=8] {'fs_0','fs_1'}, dimensions={0} | all-to-all | bytes 2097152 | tf_op jit(solution)/shard_map/all_to_all | solution.py:21
  87.6 1.2 broadcast_in_dim.16
  88.8 9.8 %all-to-all-start.2 = ((bf16[16,128,256]{2,1,0:T(8,128)(2,1)}), bf16[16,128,256]{2,1,0:T(8,128)(2,1)S(1)}, u32[]{:S(2)}, u32[]{:S(2)}) async-start(bf16[16,128,256]{2,1,0:T(8,128)(2,1)} %broadcast_in_dim.16), calls=%async_computation.2 | async-start | bytes 2097152 | tf_op jit(solution)/shard_map/all_to_all | solution.py:21
  98.6 0.1 copy.31
  98.7 21.9 %all-to-all-done.2 = bf16[16,128,256]{2,1,0:T(8,128)(2,1)S(1)} async-done(((bf16[16,128,256]{2,1,0:T(8,128)(2,1)}), bf16[16,128,256]{2,1,0:T(8,128)(2,1)S(1)}, u32[]{:S(2)}, u32[]{:S(2)}) %all-to-all-start.2) | async-done | bytes 1048608 | tf_op jit(solution)/shard_map/all_to_all | solution.py:21
  120.6 1.2 broadcast_in_dim.17
  121.7 7.9 %all-to-all-start.3 = ((bf16[16,256,128]{1,2,0:T(8,128)(2,1)}), bf16[16,256,128]{1,2,0:T(8,128)(2,1)S(1)}, u32[]{:S(2)}, u32[]{:S(2)}) async-start(bf16[16,256,128]{1,2,0:T(8,128)(2,1)} %broadcast_in_dim.17), calls=%async_computation.3 | async-start | bytes 2097152 | tf_op jit(solution)/shard_map/all_to_all | solution.py:21
  129.6 0.7 fusion.21
  130.3 21.5 %all-to-all-done.3 = bf16[16,256,128]{1,2,0:T(8,128)(2,1)S(1)} async-done(((bf16[16,256,128]{1,2,0:T(8,128)(2,1)}), bf16[16,256,128]{1,2,0:T(8,128)(2,1)S(1)}, u32[]{:S(2)}, u32[]{:S(2)}) %all-to-all-start.3) | async-done | bytes 1048608 | tf_op jit(solution)/shard_map/all_to_all | solution.py:21
  151.8 1.1 broadcast_in_dim.14
  152.9 7.8 %all-to-all-start = ((bf16[16,128,256]{2,1,0:T(8,128)(2,1)}), bf16[16,128,256]{2,1,0:T(8,128)(2,1)}, u32[]{:S(2)}, u32[]{:S(2)}) async-start(bf16[16,128,256]{2,1,0:T(8,128)(2,1)} %broadcast_in_dim.14), calls=%async_computation | async-start | bytes 2097152 | tf_op jit(solution)/shard_map/all_to_all | solution.py:21
  160.9 0.5 all-gather.14.cloned.1.call-update
  161.4 3.2 fusion
  164.6 0.3 copy-done
  164.9 1.3 fusion.13
  166.2 1.3 fusion.12
  167.5 0.3 multiply_add_fusion
  167.8 15.2 %all-to-all-done = bf16[16,128,256]{2,1,0:T(8,128)(2,1)} async-done(((bf16[16,128,256]{2,1,0:T(8,128)(2,1)}), bf16[16,128,256]{2,1,0:T(8,128)(2,1)}, u32[]{:S(2)}, u32[]{:S(2)}) %all-to-all-start) | async-done | bytes 1048608 | tf_op jit(solution)/shard_map/all_to_all | solution.py:21
  183.0 8.8 %convolution_convert_fusion = bf16[1024,2048]{1,0:T(8,128)(2,1)} fusion(bf16[256,2048]{0,1:T(8,128)(2,1)S(1)} %bitcast.55, f32[1024,256]{1,0:T(8,128)S(1)} %bitcast.58, bf16[2048,256]{1,0:T(8,128)(2,1)} %bitcast, bf16[1024,2048]{1,0:T(8,128)(2,1)} %all-gather.10.cloned.1.call-done, f32[2048]{0:T(1024)S(1)} %convert_element_type.79, ...), kind=kOutput, calls=%fused_computation.18 | convolution fusion | flops 2159017984 | bytes 11546624 | tf_op jit(solution)/shard_map/dot_general | solution.py:106
  191.8 2.5 copy.46
  194.3 56.0 %all_to_all.43 = bf16[8,1024,256]{2,1,0:T(8,128)(2,1)S(1)} all-to-all(bf16[8,1024,256]{2,1,0:T(8,128)(2,1)S(1)} %bitcast.44), channel_id=1, replica_groups=mesh['rep'=2,'fs_0'=4,'fs_1'=4,'tp'=8] {'tp'}, dimensions={0} | all-to-all | bytes 8388608 | tf_op jit(solution)/shard_map/all_to_all | solution.py:35
  250.3 0.6 convert_reduce_fusion.1
  250.9 0.2 multiply_reduce_fusion.1
  251.1 0.6 broadcast_in_dim.18
  251.8 4.2 %all-to-all-start.5 = ((f32[8,1,1024]{2,1,0:T(1,128)}), f32[8,1,1024]{2,1,0:T(1,128)S(1)}, u32[]{:S(2)}, u32[]{:S(2)}) async-start(f32[8,1,1024]{2,1,0:T(1,128)} %broadcast_in_dim.18), calls=%async_computation.5 | async-start | bytes 65536 | tf_op jit(solution)/shard_map/all_to_all | solution.py:21
  256.0 0.8 dynamic-slice_convert_fusion.1
  256.8 4.0 all-to-all-done.5
  260.8 2.5 broadcast_in_dim.19
  263.2 1.1 constant_dynamic-update-slice_fusion.7
  264.3 1.0 collective-permute-start
  265.3 6.1 %collective-permute-done = bf16[1024,256]{1,0:T(8,128)(2,1)S(1)} collective-permute-done((bf16[1024,256]{1,0:T(8,128)(2,1)S(1)}, bf16[1024,256]{1,0:T(8,128)(2,1)S(1)}, u32[]{:S(2)}, u32[]{:S(2)}) %collective-permute-start) | collective-permute-done | bytes 524320 | tf_op jit(solution)/shard_map/ppermute | solution.py:135
  271.4 2.5 collective-permute-start.2
  273.9 0.3 collective-permute-done.1
  274.2 0.7 collective-permute-start.3
  274.9 5.1 %collective-permute-done.2 = bf16[1024,256]{1,0:T(8,128)(2,1)S(1)} collective-permute-done((bf16[1024,256]{1,0:T(8,128)(2,1)S(1)}, bf16[1024,256]{1,0:T(8,128)(2,1)S(1)}, u32[]{:S(2)}, u32[]{:S(2)}) %collective-permute-start.2) | collective-permute-done | bytes 524320 | tf_op jit(solution)/shard_map/ppermute | solution.py:135
  280.0 2.5 collective-permute-start.4
  282.5 4.6 %copy.35 = bf16[4,4,1024,128]{3,2,1,0:T(8,128)(2,1)} copy(bf16[4,4,1024,128]{3,2,0,1:T(8,128)(2,1)} %bitcast.47) | data formatting | bytes 8388608 | tf_op jit(solution)/shard_map/transpose | solution.py:50
  287.1 6.4 %copy.36 = bf16[1024,16,128]{0,2,1:T(8,128)(2,1)} copy(bf16[1024,16,128]{2,0,1:T(8,128)(2,1)} %bitcast.45) | data formatting | bytes 8388608 | tf_op jit(solution)/shard_map/transpose | solution.py:14
  293.5 4.8 %copy.34 = bf16[4,4,128,1024]{3,2,1,0:T(8,128)(2,1)} copy(bf16[4,4,128,1024]{3,2,0,1:T(8,128)(2,1)} %bitcast.48) | data formatting | bytes 8388608 | tf_op jit(solution)/shard_map/transpose | solution.py:50
  298.3 2.3 collective-permute-start.5
  300.6 0.9 constant_dynamic-update-slice_fusion.6
  301.5 0.9 constant_dynamic-update-slice_fusion.5
  302.4 0.9 constant_dynamic-update-slice_fusion.4
  303.3 0.9 constant_dynamic-update-slice_fusion.3
  304.2 0.9 constant_dynamic-update-slice_fusion.2
  305.0 1.9 collective-permute-done.5
  306.9 0.9 constant_dynamic-update-slice_fusion.1
  307.8 0.9 constant_dynamic-update-slice_fusion
  308.6 3.1 fusion.3
  311.7 14.6 %convolution_convert_fusion.1 = bf16[1024,2048]{1,0:T(8,128)(2,1)} fusion(bf16[1024,2048]{0,1:T(8,128)(2,1)} %bitcast.49, bf16[2048,1024]{1,0:T(8,128)(2,1)} %bitcast.50, bf16[1024,2048]{1,0:T(8,128)(2,1)} %constant_dynamic-update-slice_fusion, f32[2048]{0:T(1024)S(1)} %convert_element_type.95, f32[1024]{0:T(1024)S(1)} %add_rsqrt_fusion.1), kind=kOutput, calls=%fused_computation.19 | convolution fusion | flops 8603566080 | bytes 16789504 | tf_op jit(solution)/shard_map/dot_general | solution.py:148
  326.4 2.5 copy.45
  328.8 57.5 %all_to_all.44 = bf16[8,1024,256]{2,1,0:T(8,128)(2,1)S(1)} all-to-all(bf16[8,1024,256]{2,1,0:T(8,128)(2,1)S(1)} %bitcast.46), channel_id=1, replica_groups=mesh['rep'=2,'fs_0'=4,'fs_1'=4,'tp'=8] {'tp'}, dimensions={0} | all-to-all | bytes 8388608 | tf_op jit(solution)/shard_map/all_to_all | solution.py:35
  386.4 0.6 convert_reduce_fusion
  386.9 0.2 multiply_reduce_fusion
  387.2 0.6 broadcast_in_dim.20
  387.8 4.3 %all-to-all-start.7 = ((f32[8,1,1024]{2,1,0:T(1,128)}), f32[8,1,1024]{2,1,0:T(1,128)S(1)}, u32[]{:S(2)}, u32[]{:S(2)}) async-start(f32[8,1,1024]{2,1,0:T(1,128)} %broadcast_in_dim.20), calls=%async_computation.7 | async-start | bytes 65536 | tf_op jit(solution)/shard_map/all_to_all | solution.py:21
  392.1 0.8 dynamic-slice_convert_fusion
  392.8 4.0 all-to-all-done.7
  396.9 1.1 add_convert_fusion
  (37 shorter events, 0.4 us)
Async XLA Ops:
  6.5 81.1 %copy-start.2 = (bf16[128,256]{1,0:T(8,128)(2,1)S(1)}, bf16[128,256]{1,0:T(8,128)(2,1)}, u32[]{:S(2)}) copy-start(bf16[128,256]{1,0:T(8,128)(2,1)} %param.16) | copy-start | bytes 196612
  6.5 39.2 %all-gather.16.cloned.1.call-start = ((), (), s32[]{:S(2)}) async-start(), calls=%async_computation.11 | async-start | bytes 1310720 | tf_op jit(solution)/shard_map/all_gather | solution.py:47
  7.3 91.3 %copy-start.4 = (bf16[256,128]{1,0:T(8,128)(2,1)S(1)}, bf16[256,128]{1,0:T(8,128)(2,1)}, u32[]{:S(2)}) copy-start(bf16[256,128]{1,0:T(8,128)(2,1)} %param.18) | copy-start | bytes 196612
  7.3 153.6 %all-gather.12.cloned.1.call-start = ((), (), s32[]{:S(2)}) async-start(), calls=%async_computation.9 | async-start | bytes 1310720 | tf_op jit(solution)/shard_map/all_gather | solution.py:47
  8.0 153.3 %all-gather.10.cloned.1.call-start = ((), (), s32[]{:S(2)}) async-start(), calls=%async_computation.8 | async-start | bytes 4718592 | tf_op jit(solution)/shard_map/all_gather | solution.py:90
  8.8 273.8 %all-gather.18.cloned.1.call-start = ((), (), s32[]{:S(2)}) async-start(), calls=%async_computation.12 | async-start | bytes 5242880 | tf_op jit(solution)/shard_map/all_gather | solution.py:47
  46.7 105.1 %copy-start.3 = (bf16[128,256]{1,0:T(8,128)(2,1)S(1)}, bf16[128,256]{1,0:T(8,128)(2,1)}, u32[]{:S(2)}) copy-start(bf16[128,256]{1,0:T(8,128)(2,1)} %param.14) | copy-start | bytes 196612
  88.8 72.0 %copy-start.5 = (bf16[2048]{0:T(1024)(128)(2,1)S(1)}, bf16[2048]{0:T(1024)(128)(2,1)}, u32[]{:S(2)}) copy-start(bf16[2048]{0:T(1024)(128)(2,1)} %param.13) | copy-start | bytes 12292
  88.8 31.8 %all-to-all-start.2 = ((bf16[16,128,256]{2,1,0:T(8,128)(2,1)}), bf16[16,128,256]{2,1,0:T(8,128)(2,1)S(1)}, u32[]{:S(2)}, u32[]{:S(2)}) async-start(bf16[16,128,256]{2,1,0:T(8,128)(2,1)} %broadcast_in_dim.16), calls=%async_computation.2 | async-start | bytes 2097152 | tf_op jit(solution)/shard_map/all_to_all | solution.py:21
  121.7 30.1 %all-to-all-start.3 = ((bf16[16,256,128]{1,2,0:T(8,128)(2,1)}), bf16[16,256,128]{1,2,0:T(8,128)(2,1)S(1)}, u32[]{:S(2)}, u32[]{:S(2)}) async-start(bf16[16,256,128]{1,2,0:T(8,128)(2,1)} %broadcast_in_dim.17), calls=%async_computation.3 | async-start | bytes 2097152 | tf_op jit(solution)/shard_map/all_to_all | solution.py:21
  152.9 30.1 %all-to-all-start = ((bf16[16,128,256]{2,1,0:T(8,128)(2,1)}), bf16[16,128,256]{2,1,0:T(8,128)(2,1)}, u32[]{:S(2)}, u32[]{:S(2)}) async-start(bf16[16,128,256]{2,1,0:T(8,128)(2,1)} %broadcast_in_dim.14), calls=%async_computation | async-start | bytes 2097152 | tf_op jit(solution)/shard_map/all_to_all | solution.py:21
  160.8 132.7 %all-gather.14.cloned.1.call-start = ((), (), s32[]{:S(2)}) async-start(), calls=%async_computation.10 | async-start | bytes 5242880 | tf_op jit(solution)/shard_map/all_gather | solution.py:47
  161.4 3.5 copy-start
  250.3 12.9 %copy-start.1 = (bf16[1024,256]{1,0:T(8,128)(2,1)S(1)}, bf16[1024,256]{1,0:T(8,128)(2,1)}, u32[]{:S(2)}) copy-start(bf16[1024,256]{1,0:T(8,128)(2,1)} %param.12) | copy-start | bytes 1572868
  250.9 31.6 %copy-start.6 = (bf16[2048]{0:T(1024)(128)(2,1)S(1)}, bf16[2048]{0:T(1024)(128)(2,1)}, u32[]{:S(2)}) copy-start(bf16[2048]{0:T(1024)(128)(2,1)} %param.20) | copy-start | bytes 12292
  251.8 9.0 %all-to-all-start.5 = ((f32[8,1,1024]{2,1,0:T(1,128)}), f32[8,1,1024]{2,1,0:T(1,128)S(1)}, u32[]{:S(2)}, u32[]{:S(2)}) async-start(f32[8,1,1024]{2,1,0:T(1,128)} %broadcast_in_dim.18), calls=%async_computation.5 | async-start | bytes 65536 | tf_op jit(solution)/shard_map/all_to_all | solution.py:21
  264.3 7.1 %collective-permute-start = (bf16[1024,256]{1,0:T(8,128)(2,1)S(1)}, bf16[1024,256]{1,0:T(8,128)(2,1)S(1)}, u32[]{:S(2)}, u32[]{:S(2)}) collective-permute-start(bf16[1024,256]{1,0:T(8,128)(2,1)S(1)} %get-tuple-element.6), channel_id=1, source_target_pairs={{0,1},{1,2},{2,3},{3,4},{4,5},{5,6},{6,7},{7,0},{8,9},{9,10},{10,1... | collective-permute-start | bytes 1572872 | tf_op jit(solution)/shard_map/ppermute | solution.py:135
  265.3 8.9 %collective-permute-start.1 = (bf16[1024,256]{1,0:T(8,128)(2,1)S(1)}, bf16[1024,256]{1,0:T(8,128)(2,1)S(1)}, u32[]{:S(2)}, u32[]{:S(2)}) collective-permute-start(bf16[1024,256]{1,0:T(8,128)(2,1)S(1)} %get-tuple-element.6), channel_id=1, source_target_pairs={{0,7},{1,0},{2,1},{3,2},{4,3},{5,4},{6,5},{7,6},{8,15},{9,8},{10,9... | collective-permute-start | bytes 1572872 | tf_op jit(solution)/shard_map/ppermute | solution.py:140
  271.4 8.6 %collective-permute-start.2 = (bf16[1024,256]{1,0:T(8,128)(2,1)S(1)}, bf16[1024,256]{1,0:T(8,128)(2,1)S(1)}, u32[]{:S(2)}, u32[]{:S(2)}) collective-permute-start(bf16[1024,256]{1,0:T(8,128)(2,1)S(1)} %collective-permute-done), channel_id=1, source_target_pairs={{0,1},{1,2},{2,3},{3,4},{4,5},{5,6},{6,7},{7,0},{8,9},{9,10},{10,1... | collective-permute-start | bytes 1572872 | tf_op jit(solution)/shard_map/ppermute | solution.py:135
  274.2 24.1 %collective-permute-start.3 = (bf16[1024,256]{1,0:T(8,128)(2,1)S(1)}, bf16[1024,256]{1,0:T(8,128)(2,1)S(1)}, u32[]{:S(2)}, u32[]{:S(2)}) collective-permute-start(bf16[1024,256]{1,0:T(8,128)(2,1)S(1)} %collective-permute-done.1), channel_id=1, source_target_pairs={{0,7},{1,0},{2,1},{3,2},{4,3},{5,4},{6,5},{7,6},{8,15},{9,8},{10,9... | collective-permute-start | bytes 1572872 | tf_op jit(solution)/shard_map/ppermute | solution.py:140
  280.0 21.4 %collective-permute-start.4 = (bf16[1024,256]{1,0:T(8,128)(2,1)S(1)}, bf16[1024,256]{1,0:T(8,128)(2,1)S(1)}, u32[]{:S(2)}, u32[]{:S(2)}) collective-permute-start(bf16[1024,256]{1,0:T(8,128)(2,1)S(1)} %collective-permute-done.2), channel_id=1, source_target_pairs={{0,1},{1,2},{2,3},{3,4},{4,5},{5,6},{6,7},{7,0},{8,9},{9,10},{10,1... | collective-permute-start | bytes 1572872 | tf_op jit(solution)/shard_map/ppermute | solution.py:135
  298.3 8.6 %collective-permute-start.5 = (bf16[1024,256]{1,0:T(8,128)(2,1)S(1)}, bf16[1024,256]{1,0:T(8,128)(2,1)S(1)}, u32[]{:S(2)}, u32[]{:S(2)}) collective-permute-start(bf16[1024,256]{1,0:T(8,128)(2,1)S(1)} %collective-permute-done.3), channel_id=1, source_target_pairs={{0,7},{1,0},{2,1},{3,2},{4,3},{5,4},{6,5},{7,6},{8,15},{9,8},{10,9... | collective-permute-start | bytes 1572872 | tf_op jit(solution)/shard_map/ppermute | solution.py:140
  301.5 6.3 %collective-permute-start.6 = (bf16[1024,256]{1,0:T(8,128)(2,1)S(1)}, bf16[1024,256]{1,0:T(8,128)(2,1)S(1)}, u32[]{:S(2)}, u32[]{:S(2)}) collective-permute-start(bf16[1024,256]{1,0:T(8,128)(2,1)S(1)} %collective-permute-done.4), channel_id=1, source_target_pairs={{0,1},{1,2},{2,3},{3,4},{4,5},{5,6},{6,7},{7,0},{8,9},{9,10},{10,1... | collective-permute-start | bytes 1572872 | tf_op jit(solution)/shard_map/ppermute | solution.py:135
  387.8 9.0 %all-to-all-start.7 = ((f32[8,1,1024]{2,1,0:T(1,128)}), f32[8,1,1024]{2,1,0:T(1,128)S(1)}, u32[]{:S(2)}, u32[]{:S(2)}) async-start(f32[8,1,1024]{2,1,0:T(1,128)} %broadcast_in_dim.20), calls=%async_computation.7 | async-start | bytes 65536 | tf_op jit(solution)/shard_map/all_to_all | solution.py:21
Sparse Core Ops, SparseCore 0:
  9.1 36.5 all-gather.15
  47.5 43.0 all-gather.11
  92.5 42.0 all-gather.9
  136.3 63.2 all-gather.17
  201.2 50.9 all-gather.13
